TPU v7x, 32 devices: a whole 2x2x4 slice. The times are simulated.
32 devices in a mesh: ra: 4 (over z), cb: 4 (over y, x), dp: 2 (over core).
Axes of the slice: x: 2, y: 2, z: 4, core: 2. Of those that a mesh axis runs over, the one named last changes fastest.
Arguments:
- tokens: bfloat16 [3072, 4096], P('dp', 'ra'), may hold values from -20 to 20
- pre_gain: float32 [4096], P('ra'), may hold values from 0.1 to 1.9
- up_weight: bfloat16 [4096, 16384], P('ra', 'cb'), may hold values from -0.09375 to 0.09375
- up_bias: float32 [16384], P('cb'), may hold values from -4 to 4
- down_weight: bfloat16 [16384, 4096], P('cb', 'ra'), may hold values from -0.046875 to 0.046875
- post_gain: float32 [4096], P('ra'), may hold values from 0.1 to 1.9
Outputs:
- stream_out: bfloat16 [3072, 4096], P('dp', 'ra')
All inputs are finite; a program needn't handle non-finite values.
Results may differ from a plain program's by a relative error of at most 0.0051.
Values may be sent and summed in bfloat16 or wider, within the bound.
A program may use at most 128 MiB of HBM per device.

v0:
```python
import jax
import jax.numpy as jnp
from jax import lax
from jax.sharding import PartitionSpec as P

D = 4096
epsilon = 1e-06
residual_weight = 0.5


def activate(summed, inverse, offset):
    return jnp.square(jax.nn.relu(summed * inverse[:, None] + offset)).astype(jnp.bfloat16)


def body(tokens, pre_gain, up_weight, up_bias, down_weight, post_gain):
    stream = tokens.astype(jnp.float32)
    energy = jnp.sum(stream * stream, axis=1)
    scaled = (stream * pre_gain).astype(jnp.bfloat16)
    partial_value = jnp.dot(scaled, up_weight, preferred_element_type=jnp.float32)
    total = lax.psum(energy, "ra")
    share = lax.psum_scatter(partial_value, "ra", scatter_dimension=1, tiled=True)
    width = share.shape[1]
    offset = lax.dynamic_slice_in_dim(up_bias, lax.axis_index("ra") * width, width, 0)
    hidden = activate(share, lax.rsqrt(total / D + epsilon), offset)
    branch = jnp.dot(
        lax.all_gather(hidden, "ra", axis=1, tiled=True),
        down_weight,
        preferred_element_type=jnp.float32,
    )
    branch = lax.psum(branch, "cb")
    branch_energy = lax.psum(jnp.sum(branch * branch, axis=1), "ra")
    normed = branch * lax.rsqrt(branch_energy / D + epsilon)[:, None] * post_gain
    return (residual_weight * stream + normed).astype(jnp.bfloat16)


def solution(mesh):
    in_specs = (P("dp", "ra"), P("ra"), P("ra", "cb"), P("cb"), P("cb", "ra"), P("ra"))
    out_specs = P("dp", "ra")
    return jax.shard_map(body, mesh=mesh, in_specs=in_specs, out_specs=out_specs, check_vma=False)
```

profile of v0, /device:TPU:0, one launch (start us, length us, event | category | flops | bytes accessed | tf_op | source)
XLA Modules:
  0.0 853.5 jit_solution(10800701514293128842)
XLA Ops:
  6.5 0.0 reduce-scatter.2.cloned.1.call-start
  6.5 21.1 %fusion.4 = f32[1536,4096]{1,0:T(8,128)} fusion(bf16[1024,4096]{1,0:T(8,128)(2,1)} %param.8, bf16[1536,1024]{1,0:T(8,128)(2,1)} %param.6, f32[1024]{0:T(1024)} %param.7), kind=kOutput, calls=%fused_computation.9 | convolution fusion | flops 12889620480 | bytes 36704256 | tf_op jit(solution)/shard_map/dot_general | solution.py:19
  27.7 0.0 copy-start
  27.7 0.0 reduce-scatter.2.cloned.1.call-update
  27.7 0.0 all-gather.2.cloned.1.call-start
  27.8 0.8 dynamic_slice.3
  28.6 1.0 copy-done
  29.6 0.7 fusion.3
  30.3 14.3 %psum.21 = f32[1536]{0:T(1024)S(1)} all-reduce(f32[1536]{0:T(1024)S(1)} %fusion.3), channel_id=1, replica_groups=mesh['ra'=4,'cb'=4,'dp'=2] {'ra'}, use_global_device_ids=true, to_apply=%region_2.0 | all-reduce | flops 1536 | bytes 12288 | tf_op jit(solution)/shard_map/psum | solution.py:20
  44.6 400.5 %reduce-scatter.2.cloned.1.call-done = f32[1536,1024]{1,0:T(8,128)} async-done(((f32[1536,4096]{1,0:T(8,128)}), f32[1536,1024]{1,0:T(8,128)}) %reduce-scatter.2.cloned.1.call-update) | async-done | bytes 6291472 | tf_op jit(solution)/shard_map/reduce_scatter | solution.py:21
  445.2 5.4 multiply_convert_fusion
  450.6 0.0 all-gather.2.cloned.1.call-update
  450.6 0.0 all-reduce.2.cloned.1.call-start
  450.7 220.3 %all-gather.2.cloned.1.call-done = bf16[1536,4096]{1,0:T(8,128)(2,1)} async-done(((bf16[1536,1024]{1,0:T(8,128)(2,1)}), bf16[1536,4096]{1,0:T(8,128)(2,1)}) %all-gather.2.cloned.1.call-update) | async-done | bytes 12582928 | tf_op jit(solution)/shard_map/all_gather | solution.py:26
  671.0 19.5 %fusion.7 = f32[1536,1024]{1,0:T(8,128)} fusion(bf16[1536,4096]{1,0:T(8,128)(2,1)} %all-gather.2.cloned.1.call-done, bf16[4096,1024]{1,0:T(8,128)(2,1)} %param.10), kind=kOutput, calls=%fused_computation.13 | convolution fusion | flops 12884901888 | bytes 27262976 | tf_op jit(solution)/shard_map/dot_general | solution.py:25
  690.5 0.0 copy-start.1
  690.5 0.0 all-reduce.2.cloned.1.call-update
  690.5 136.5 %all-reduce.2.cloned.1.call-done = f32[1536,1024]{1,0:T(8,128)} async-done(((f32[1536,1024]{1,0:T(8,128)}), f32[1536,1024]{1,0:T(8,128)}) %all-reduce.2.cloned.1.call-update) | async-done | bytes 6291472 | tf_op jit(solution)/shard_map/psum | solution.py:30
  827.0 3.3 multiply_reduce_fusion
  830.3 11.9 %psum.23 = f32[1536]{0:T(1024)S(1)} all-reduce(f32[1536]{0:T(1024)S(1)} %multiply_reduce_fusion), channel_id=1, replica_groups=mesh['ra'=4,'cb'=4,'dp'=2] {'ra'}, use_global_device_ids=true, to_apply=%region_5.6 | all-reduce | flops 1536 | bytes 12288 | tf_op jit(solution)/shard_map/psum | solution.py:31
  842.3 0.0 copy-done.1
  842.3 4.7 fusion.1
  (2 shorter events, 0.0 us)
Async XLA Ops:
  6.5 438.6 %reduce-scatter.2.cloned.1.call-start = ((), (), s32[]{:S(2)}) async-start(), calls=%async_computation.1 | async-start | bytes 31457280 | tf_op jit(solution)/shard_map/reduce_scatter | solution.py:21
  27.7 1.9 copy-start
  27.7 643.3 %all-gather.2.cloned.1.call-start = ((), (), s32[]{:S(2)}) async-start(), calls=%async_computation.2 | async-start | bytes 15728640 | tf_op jit(solution)/shard_map/all_gather | solution.py:26
  450.6 376.4 %all-reduce.2.cloned.1.call-start = ((), (), s32[]{:S(2)}) async-start(), calls=%async_computation.3 | async-start | bytes 12582912 | tf_op jit(solution)/shard_map/psum | solution.py:30
  690.5 151.8 %copy-start.1 = (f32[1024]{0:T(1024)S(1)}, f32[1024]{0:T(1024)}, u32[]{:S(2)}) copy-start(f32[1024]{0:T(1024)} %param.11) | copy-start | bytes 12292
Sparse Core Ops, SparseCore 0:
  27.8 417.2 reduce-scatter.1
  450.7 220.2 all-gather.1
  690.6 136.3 all-reduce.1
where the time goes:
time: 854 us
  waiting for transfers between devices  757 us (89%)
  matrix products  40.6 us (5%)
  blocking collectives  26.3 us (3%)
  other arithmetic  14.1 us (2%)
  between operations  13.2 us (2%)
    reduce_scatter x1, waiting for transfers between devices, body(): lax.psum_scatter(partial_value, 'ra', scatter_dimension=1, tiled=True)  401 us
    all_gather x1, waiting for transfers between devices, body(): lax.all_gather(hidden, 'ra', axis=1, tiled=True)  220 us
    psum x1, waiting for transfers between devices, body(): branch = lax.psum(branch, 'cb')  137 us
    dot_general x1, matrix products, body(): jnp.dot(scaled, up_weight, preferred_element_type=jnp.float32)  21.1 us
    dot_general x1, matrix products, body(): jnp.dot(lax.all_gather(hidden, 'ra', axis=1, tiled=True), down_weight, pr...  19.5 us
  transfers between devices with their start and end apart: 3, of which 3 were waited for; matrix products, arithmetic and copies ran while one was open for 0% of the time, Pallas kernels for 0%

commit v1 on v0

--- a/solution.py
+++ b/solution.py
@@ -27,7 +27,7 @@
         down_weight,
         preferred_element_type=jnp.float32,
     )
-    branch = lax.psum(branch, "cb")
+    branch = jnp.sum(lax.all_gather(branch, "cb"), axis=0)
     branch_energy = lax.psum(jnp.sum(branch * branch, axis=1), "ra")
     normed = branch * lax.rsqrt(branch_energy / D + epsilon)[:, None] * post_gain
     return (residual_weight * stream + normed).astype(jnp.bfloat16)

time: 854 us -> 956 us (1.12)
  waiting for transfers between devices: 757 us -> 847 us
  other arithmetic: 14.1 us -> 27 us
    all_gather x0 -> x1, waiting for transfers between devices: none -> 226 us  [body(): branch = jnp.sum(lax.all_gather(branch, 'cb'), axis=0)]
    psum x1 -> x0, waiting for transfers between devices: 137 us -> none  [body(): branch = lax.psum(branch, 'cb')]
    reduce_sum x0 -> x1, other arithmetic: none -> 12.9 us  [body(): branch = jnp.sum(lax.all_gather(branch, 'cb'), axis=0)]
where the time goes in v1:
time: 956 us
  waiting for transfers between devices  847 us (89%)
  matrix products  40.7 us (4%)
  other arithmetic  27 us (3%)
  blocking collectives  26.3 us (3%)
  between operations  13.2 us (1%)
    reduce_scatter x1, waiting for transfers between devices, body(): lax.psum_scatter(partial_value, 'ra', scatter_dimension=1, tiled=True)  401 us
    all_gather x1, waiting for transfers between devices, body(): branch = jnp.sum(lax.all_gather(branch, 'cb'), axis=0)  226 us
    all_gather x1, waiting for transfers between devices, body(): lax.all_gather(hidden, 'ra', axis=1, tiled=True)  220 us
    dot_general x1, matrix products, body(): jnp.dot(scaled, up_weight, preferred_element_type=jnp.float32)  21.1 us
    dot_general x1, matrix products, body(): jnp.dot(lax.all_gather(hidden, 'ra', axis=1, tiled=True), down_weight, pr...  19.5 us
  transfers between devices with their start and end apart: 3, of which 3 were waited for; matrix products, arithmetic and copies ran while one was open for 0% of the time, Pallas kernels for 0%

profile of v1, /device:TPU:0, one launch (start us, length us, event | category | flops | bytes accessed | tf_op | source)
XLA Modules:
  0.0 955.9 jit_solution(27130960487670077)
XLA Ops:
  6.5 0.0 reduce-scatter.2.cloned.1.call-start
  6.5 21.1 %fusion.4 = f32[1536,4096]{1,0:T(8,128)} fusion(bf16[1024,4096]{1,0:T(8,128)(2,1)} %param.8, bf16[1536,1024]{1,0:T(8,128)(2,1)} %param.6, f32[1024]{0:T(1024)} %param.7), kind=kOutput, calls=%fused_computation.9 | convolution fusion | flops 12889620480 | bytes 36704256 | tf_op jit(solution)/shard_map/dot_general | solution.py:19
  27.7 0.0 copy-start
  27.7 0.0 reduce-scatter.2.cloned.1.call-update
  27.7 0.0 all-gather.4.cloned.1.call-start
  27.8 0.8 dynamic_slice.3
  28.6 1.0 copy-done
  29.6 0.7 fusion.3
  30.3 14.4 %psum.14 = f32[1536]{0:T(1024)S(1)} all-reduce(f32[1536]{0:T(1024)S(1)} %fusion.3), channel_id=1, replica_groups=mesh['ra'=4,'cb'=4,'dp'=2] {'ra'}, use_global_device_ids=true, to_apply=%region_2.0 | all-reduce | flops 1536 | bytes 12288 | tf_op jit(solution)/shard_map/psum | solution.py:20
  44.7 400.5 %reduce-scatter.2.cloned.1.call-done = f32[1536,1024]{1,0:T(8,128)} async-done(((f32[1536,4096]{1,0:T(8,128)}), f32[1536,1024]{1,0:T(8,128)}) %reduce-scatter.2.cloned.1.call-update) | async-done | bytes 6291472 | tf_op jit(solution)/shard_map/reduce_scatter | solution.py:21
  445.2 5.4 multiply_convert_fusion
  450.6 0.0 all-gather.4.cloned.1.call-update
  450.6 0.2 all-gather.6.cloned.1.call-start
  450.9 220.2 %all-gather.4.cloned.1.call-done = bf16[1536,4096]{1,0:T(8,128)(2,1)} async-done(((bf16[1536,1024]{1,0:T(8,128)(2,1)}), bf16[1536,4096]{1,0:T(8,128)(2,1)}) %all-gather.4.cloned.1.call-update) | async-done | bytes 12582928 | tf_op jit(solution)/shard_map/all_gather | solution.py:26
  671.0 19.5 %fusion.7 = f32[1536,1024]{1,0:T(8,128)} fusion(bf16[1536,4096]{1,0:T(8,128)(2,1)} %all-gather.4.cloned.1.call-done, bf16[4096,1024]{1,0:T(8,128)(2,1)} %param.10), kind=kOutput, calls=%fused_computation.13 | convolution fusion | flops 12884901888 | bytes 27262976 | tf_op jit(solution)/shard_map/dot_general | solution.py:25
  690.5 0.0 all-gather.6.cloned.1.call-update
  690.5 225.9 %all-gather.6.cloned.1.call-done = f32[6144,1024]{1,0:T(8,128)} async-done(((f32[1536,1024]{1,0:T(8,128)}), f32[6144,1024]{1,0:T(8,128)}) %all-gather.6.cloned.1.call-update) | async-done | bytes 25165840 | tf_op jit(solution)/shard_map/all_gather | solution.py:30
  916.5 12.9 %reduce_sum.28 = f32[1536,1024]{1,0:T(8,128)} reduce(f32[4,1536,1024]{2,1,0:T(8,128)} %bitcast.4, f32[]{:T(128)} %constant.9.clone.1), dimensions={0}, to_apply=%region_3.4 | reduce | flops 4718592 | bytes 31457284 | tf_op jit(solution)/shard_map/reduce_sum | solution.py:30
  929.4 0.0 copy-start.1
  929.4 3.3 multiply_reduce_fusion
  932.6 11.9 %psum.15 = f32[1536]{0:T(1024)S(1)} all-reduce(f32[1536]{0:T(1024)S(1)} %multiply_reduce_fusion), channel_id=1, replica_groups=mesh['ra'=4,'cb'=4,'dp'=2] {'ra'}, use_global_device_ids=true, to_apply=%region_5.6 | all-reduce | flops 1536 | bytes 12288 | tf_op jit(solution)/shard_map/psum | solution.py:31
  944.6 0.0 copy-done.1
  944.6 4.7 fusion.1
  (2 shorter events, 0.0 us)
Async XLA Ops:
  6.5 438.6 %reduce-scatter.2.cloned.1.call-start = ((), (), s32[]{:S(2)}) async-start(), calls=%async_computation.1 | async-start | bytes 31457280 | tf_op jit(solution)/shard_map/reduce_scatter | solution.py:21
  27.7 1.9 copy-start
  27.7 643.3 %all-gather.4.cloned.1.call-start = ((), (), s32[]{:S(2)}) async-start(), calls=%async_computation.2 | async-start | bytes 15728640 | tf_op jit(solution)/shard_map/all_gather | solution.py:26
  450.6 465.8 %all-gather.6.cloned.1.call-start = ((), (), s32[]{:S(2)}) async-start(), calls=%async_computation.3 | async-start | bytes 31457280 | tf_op jit(solution)/shard_map/all_gather | solution.py:30
  929.4 15.2 %copy-start.1 = (f32[1024]{0:T(1024)S(1)}, f32[1024]{0:T(1024)}, u32[]{:S(2)}) copy-start(f32[1024]{0:T(1024)} %param.11) | copy-start | bytes 12292
Sparse Core Ops, SparseCore 0:
  27.8 417.2 reduce-scatter.1
  450.7 220.2 all-gather.3
  690.7 225.7 all-gather.5
